TPU v7x, 32 devices: a whole 2x2x4 slice. The times are simulated.
32 devices in a mesh: ep: 8 (over z, x), tp: 4 (over y, core).
Axes of the slice: x: 2, y: 2, z: 4, core: 2. Of those that a mesh axis runs over, the one named last changes fastest.
Arguments:
- mixer_in: bfloat16 [1024, 2048], P('ep'), may hold values from -6 to 6
- mixer_gain: float32 [2048], replicated, may hold values from 0.1 to 1.9
- w_value: bfloat16 [2048, 1536], P(None, 'tp'), may hold values from -0.125 to 0.125
- w_gate: bfloat16 [2048, 1536], P(None, 'tp'), may hold values from -0.125 to 0.125
- w_taps: float32 [31, 1536], P(None, 'tp'), may hold values from -3 to 3
- channel_gain: float32 [1536], P('tp'), may hold values from 0.1 to 1.9
- w_output: bfloat16 [1536, 2048], P('tp'), may hold values from -0.15625 to 0.15625
- expert_in: bfloat16 [1024, 2048], P('ep'), may hold values from -6 to 6
- expert_gain: float32 [2048], replicated, may hold values from 0 to 8
- route_experts: int32 [1024, 4], P('ep'), may hold values from 0 to 7, all different within a row; in each aligned block of 128 rows (0 to 127, 128 to 255, ...) at most 128 rows name the same one
- route_scores: float32 [1024, 4], P('ep'), may hold values from -6 to 6
- expert_gate: bfloat16 [8, 2048, 2048], P('ep', None, 'tp'), may hold values from -0.125 to 0.125
- expert_up: bfloat16 [8, 2048, 2048], P('ep', None, 'tp'), may hold values from -0.125 to 0.125
- expert_down: bfloat16 [8, 2048, 2048], P('ep', 'tp'), may hold values from -0.125 to 0.125
Outputs:
- mixer_out: bfloat16 [1024, 2048], P('ep')
- expert_out: bfloat16 [1024, 2048], P('ep')
Inputs may be any that keep to these rules, and one draw needn't show every extreme that they name: `route_experts`: each row names 4 different experts. In each aligned block of 128 rows (the rows of one index of ep) no expert is named more than 128 times, a bound that some block reaches.
All inputs are finite; a program needn't handle non-finite values.
Results may differ from a plain program's by a relative error of at most 0.02.
Values may be sent and summed in bfloat16 or wider, within the bound.
A program may use at most 64 MiB of HBM per device.

v0:
```python
import jax
import jax.numpy as jnp
from jax import lax
from jax.sharding import PartitionSpec as P

CONV_CH = 1536
CONV_W = 31
TOP_K = 4
epsilon = 1e-05
clamp_limit = 7.0
swish_slope = 1.702


def shifted(block, axis, distance):
    devices = range(lax.axis_size(axis))
    route = [(i - distance, i) for i in devices if i - distance in devices]
    return lax.ppermute(block, axis, route)


def row_norm(inputs, gains):
    widened = inputs.astype(jnp.float32)
    row_mean = jnp.mean(widened, axis=-1, keepdims=True)
    row_var = jnp.mean(jnp.square(widened - row_mean), axis=-1, keepdims=True)
    return (widened - row_mean) * lax.rsqrt(row_var + epsilon) * gains


def local(
    mixer_in,
    mixer_gain,
    w_value,
    w_gate,
    w_taps,
    channel_gain,
    w_output,
    expert_in,
    expert_gain,
    route_experts,
    route_scores,
    expert_gate,
    expert_up,
    expert_down,
):
    normed = row_norm(mixer_in, mixer_gain).astype(jnp.bfloat16)
    values = jnp.dot(normed, w_value, preferred_element_type=jnp.float32)
    gate_pre = jnp.dot(normed, w_gate, preferred_element_type=jnp.float32)
    gated_values = (values * jax.nn.sigmoid(gate_pre)).astype(jnp.bfloat16)
    mixer_rows = gated_values.shape[0]
    reach_rows = CONV_W - 1
    earlier = shifted(gated_values[mixer_rows - reach_rows :], "ep", 1)
    extended = jnp.concatenate([earlier, gated_values], axis=0)
    conv_out = jnp.zeros(gated_values.shape, jnp.float32)
    for offset in range(CONV_W):
        conv_out = (
            conv_out + extended[offset : offset + mixer_rows].astype(jnp.float32) * w_taps[offset]
        )
    channel_sums = lax.psum(
        (
            jnp.sum(conv_out, axis=1, keepdims=True),
            jnp.sum(conv_out * conv_out, axis=1, keepdims=True),
        ),
        "tp",
    )
    row_mean = channel_sums[0] / CONV_CH
    row_var = channel_sums[1] / CONV_CH - row_mean * row_mean
    activated = jax.nn.silu(
        (conv_out - row_mean) * lax.rsqrt(row_var + epsilon) * channel_gain
    ).astype(jnp.bfloat16)
    mixer_out = lax.psum(
        jnp.dot(activated, w_output, preferred_element_type=jnp.float32).astype(jnp.bfloat16), "tp"
    )
    rows_b = expert_in.shape[0]
    width = expert_in.shape[1]
    experts = lax.axis_size("ep")
    capacity = 2 * rows_b * TOP_K // experts
    slot_share = capacity // lax.axis_size("tp")
    column = lax.axis_index("tp")
    normed_b = row_norm(expert_in, expert_gain).astype(jnp.bfloat16)
    raised = jnp.exp(route_scores)
    route_weights = raised / jnp.sum(raised, axis=1, keepdims=True)
    flat_ids = route_experts.reshape(-1)
    onehot = (flat_ids[:, None] == jnp.arange(experts, dtype=jnp.int32)[None, :]).astype(jnp.int32)
    slot_index = jnp.sum((jnp.cumsum(onehot, axis=0) - onehot) * onehot, axis=1)
    owner_row = jnp.arange(rows_b * TOP_K, dtype=jnp.int32) // TOP_K
    slot_table = (
        jnp.full((capacity * experts,), rows_b, jnp.int32)
        .at[slot_index * experts + flat_ids]
        .set(owner_row)
    )
    padded = jnp.concatenate([normed_b, jnp.zeros((1, width), jnp.bfloat16)], axis=0)
    gate_w = expert_gate[0]
    up_w = expert_up[0]
    down_w = expert_down[0]
    own_table = lax.dynamic_slice_in_dim(
        slot_table, column * slot_share * experts, slot_share * experts
    )
    sending = jnp.take(padded, own_table, axis=0).reshape(slot_share, experts, width)
    arrived = lax.all_to_all(sending, "ep", split_axis=1, concat_axis=1, tiled=True)
    block_rows = lax.all_gather(arrived, "tp", axis=0, tiled=True)
    flat_rows = block_rows.reshape(block_rows.shape[0] * block_rows.shape[1], block_rows.shape[2])
    gate_e = jnp.minimum(
        jnp.dot(flat_rows, gate_w, preferred_element_type=jnp.float32), clamp_limit
    )
    up_e = jnp.clip(
        jnp.dot(flat_rows, up_w, preferred_element_type=jnp.float32), -clamp_limit, clamp_limit
    )
    hidden = (
        ((up_e + 1.0) * gate_e * jax.nn.sigmoid(swish_slope * gate_e))
        .astype(jnp.bfloat16)
        .reshape(block_rows.shape[0], block_rows.shape[1], gate_w.shape[1])
        .reshape(capacity * experts, gate_w.shape[1])
    )
    summed = lax.psum_scatter(
        jnp.dot(hidden, down_w, preferred_element_type=jnp.float32).astype(jnp.bfloat16),
        "tp",
        scatter_dimension=0,
        tiled=True,
    )
    returned = lax.all_to_all(
        summed.reshape(slot_share, experts, width), "ep", split_axis=1, concat_axis=1, tiled=True
    )
    every_slot = lax.all_gather(returned, "tp", axis=0, tiled=True).reshape(
        capacity * experts, width
    )
    picked = jnp.take(every_slot, slot_index * experts + flat_ids, axis=0)
    picked = picked.reshape(rows_b, TOP_K, width).astype(jnp.float32)
    expert_out = jnp.sum(picked * route_weights[:, :, None], axis=1).astype(jnp.bfloat16)
    return (mixer_out, expert_out)


def solution(mesh):
    in_specs = (
        P("ep", None),
        P(),
        P(None, "tp"),
        P(None, "tp"),
        P(None, "tp"),
        P("tp"),
        P("tp", None),
        P("ep", None),
        P(),
        P("ep", None),
        P("ep", None),
        P("ep", None, "tp"),
        P("ep", None, "tp"),
        P("ep", "tp", None),
    )
    out_specs = (P("ep", None), P("ep", None))
    return jax.shard_map(local, mesh=mesh, in_specs=in_specs, out_specs=out_specs, check_vma=False)
```

profile of v0, /device:TPU:0, one launch (start us, length us, event | category | flops | bytes accessed | tf_op | source)
XLA Modules:
  0.0 263.1 jit_solution(18099323295168561547)
XLA Ops:
  10.0 2.4 scatter_custom_fusion
  13.8 1.3 fusion.24
  15.3 1.4 fusion.26
  16.8 2.3 gather_fusion
  19.1 2.4 copy_select_fusion
  21.6 32.8 %all_to_all.10 = bf16[32,8,2048]{2,0,1:T(8,128)(2,1)S(1)} all-to-all(bf16[32,8,2048]{2,0,1:T(8,128)(2,1)S(1)} %copy_select_fusion), channel_id=1, replica_groups=mesh['ep'=8,'tp'=4] {'ep'}, dimensions={1} | all-to-all | bytes 2097152 | tf_op jit(solution)/shard_map/all_to_all | solution.py:97
  54.4 1.6 copy.40
  56.0 33.6 %all-gather.3.cloned.1.call-done = bf16[128,8,2048]{2,1,0:T(8,128)(2,1)} async-done(((bf16[32,8,2048]{2,1,0:T(8,128)(2,1)}), bf16[128,8,2048]{2,1,0:T(8,128)(2,1)}) %all-gather.3.cloned.1.call-update) | async-done | bytes 4194320 | tf_op jit(solution)/shard_map/all_gather | solution.py:98
  89.7 6.6 %fusion.2 = f32[1024,512]{1,0:T(8,128)} fusion(bf16[128,8,2048]{2,1,0:T(8,128)(2,1)} %all-gather.3.cloned.1.call-done, bf16[1,2048,512]{2,1,0:T(8,128)(2,1)} %param.26), kind=kOutput, calls=%fused_computation.5 | convolution fusion | flops 2147483648 | bytes 8388608 | tf_op jit(solution)/shard_map/dot_general | solution.py:104
  96.2 10.3 %convolution_convert_fusion = bf16[1024,2048]{1,0:T(8,128)(2,1)} fusion(bf16[1,512,2048]{2,1,0:T(8,128)(2,1)S(1)} %copy-done, f32[1024,512]{1,0:T(8,128)} %fusion.2, bf16[1,2048,512]{2,1,0:T(8,128)(2,1)} %param.25, bf16[128,8,2048]{2,1,0:T(8,128)(2,1)} %all-gather.3.cloned.1.call-done), kind=kOutput, calls=%fused_computation.8 | convolution fusion | flops 4302307328 | bytes 14680064 | tf_op jit(solution)/shard_map/dot_general | solution.py:113
  106.6 44.7 %reduce-scatter.2.cloned.1.call-done = bf16[256,2048]{1,0:T(8,128)(2,1)} async-done(((bf16[1024,2048]{1,0:T(8,128)(2,1)}), bf16[256,2048]{1,0:T(8,128)(2,1)}) %reduce-scatter.2.cloned.1.call-update) | async-done | bytes 1048592 | tf_op jit(solution)/shard_map/reduce_scatter | solution.py:112
  151.3 1.8 copy.41
  153.1 30.9 %all_to_all.11 = bf16[32,8,2048]{2,0,1:T(8,128)(2,1)S(1)} all-to-all(bf16[32,8,2048]{2,0,1:T(8,128)(2,1)S(1)} %copy.41), channel_id=1, replica_groups=mesh['ep'=8,'tp'=4] {'ep'}, dimensions={1} | all-to-all | bytes 2097152 | tf_op jit(solution)/shard_map/all_to_all | solution.py:118
  184.0 1.6 copy.42
  186.3 1.9 fusion.81
  188.9 3.4 %collective-permute-start = (bf16[30,384]{1,0:T(8,128)(2,1)S(1)}, bf16[30,384]{1,0:T(8,128)(2,1)S(1)}, u32[]{:S(2)}, u32[]{:S(2)}) collective-permute-start(bf16[30,384]{1,0:T(8,128)(2,1)S(1)} %slice.260), channel_id=1, source_target_pairs={{0,4},{4,8},{8,12},{12,16},{16,20},{20,24},{24,28},{1,5},{5,9},{9,... | collective-permute-start | bytes 69128 | tf_op jit(solution)/shard_map/ppermute | solution.py:17
  194.7 6.5 %all-reduce.1 = (f32[128,1]{0,1:T(1,128)S(1)}, f32[128,1]{0,1:T(1,128)S(1)}) all-reduce(f32[128,1]{0,1:T(1,128)S(1)} %bitcast.51, f32[128,1]{0,1:T(1,128)S(1)} %bitcast.50), channel_id=1, replica_groups=mesh['ep'=8,'tp'=4] {'tp'}, use_global_device_ids=true, to_apply=%region_5.0 | all-reduce | flops 256 | bytes 2048 | tf_op jit(solution)/shard_map/psum | solution.py:56
  201.1 2.7 %convolution_convert_fusion.1 = bf16[128,2048]{1,0:T(8,128)(2,1)} fusion(bf16[384,2048]{1,0:T(8,128)(2,1)} %param.20, f32[128,384]{1,0:T(8,128)S(1)} %get-tuple-element.39, f32[384]{0:T(512)S(1)} %copy-done.7, f32[128]{0:T(128)S(1)} %get-tuple-element.41, f32[128]{0:T(128)S(1)} %get-tuple-element.40), kind=kOutput, calls=%fused_computation.9 | convolution fusion | flops 201981952 | bytes 2296320 | tf_op jit(solution)/shard_map/dot_general | solution.py:69
  203.9 14.5 %all-gather.5.cloned.1.call-done = bf16[128,8,2048]{2,1,0:T(8,128)(2,1)} async-done(((bf16[32,8,2048]{2,1,0:T(8,128)(2,1)}), bf16[128,8,2048]{2,1,0:T(8,128)(2,1)}) %all-gather.5.cloned.1.call-update) | async-done | bytes 4194320 | tf_op jit(solution)/shard_map/all_gather | solution.py:121
  218.4 8.0 %gather_fusion.1 = bf16[512,2048]{1,0:T(8,128)(2,1)} fusion(bf16[1024,2048]{1,0:T(8,128)(2,1)} %bitcast.44, s32[1024]{0:T(1024)S(1)} %pad_clamp_fusion), kind=kCustom, calls=%fused_computation.1 | custom fusion | bytes 4196352 | tf_op jit(solution)/shard_map/jit(_take)/gather | solution.py:124
  226.4 4.1 %gather.15 = bf16[128,4,2048]{2,1,0:T(4,128)(2,1)} reshape(bf16[512,2048]{1,0:T(8,128)(2,1)} %gather_fusion.1) | data formatting | bytes 4194304 | tf_op jit(solution)/shard_map/jit(_take)/gather | solution.py:124
  230.6 6.4 %multiply_reduce_fusion = bf16[128,2048]{1,0:T(8,128)(2,1)} fusion(f32[128,4]{1,0:T(8,128)S(1)} %copy.43, bf16[128,4,2048]{2,1,0:T(4,128)(2,1)} %gather.15, pred[128,4]{1,0:T(8,128)(4,1)S(1)} %copy.36), kind=kLoop, calls=%fused_computation.7 | loop fusion | flops 3932160 | bytes 2624000 | tf_op jit(solution)/shard_map/reduce_sum | solution.py:126
  237.0 17.7 %all-reduce.4.cloned.1.call-done = bf16[128,2048]{1,0:T(8,128)(2,1)} async-done(((bf16[128,2048]{1,0:T(8,128)(2,1)}), bf16[128,2048]{1,0:T(8,128)(2,1)}) %all-reduce.4.cloned.1.call-update) | async-done | bytes 524304 | tf_op jit(solution)/shard_map/psum | solution.py:68
  254.7 1.9 copy.46
  (64 shorter events, 8.1 us)
Async XLA Ops:
  7.2 89.1 %copy-start = (bf16[1,512,2048]{2,1,0:T(8,128)(2,1)S(1)}, bf16[1,512,2048]{2,1,0:T(8,128)(2,1)}, u32[]{:S(2)}) copy-start(bf16[1,512,2048]{2,1,0:T(8,128)(2,1)} %param.27) | copy-start | bytes 6291460
  7.2 82.5 %all-gather.3.cloned.1.call-start = ((), (), s32[]{:S(2)}) async-start(), calls=%async_computation.4 | async-start | bytes 5242880 | tf_op jit(solution)/shard_map/all_gather | solution.py:98
  56.0 95.3 %reduce-scatter.2.cloned.1.call-start = ((), (), s32[]{:S(2)}) async-start(), calls=%async_computation.5 | async-start | bytes 5242880 | tf_op jit(solution)/shard_map/reduce_scatter | solution.py:112
  106.6 111.9 %all-gather.5.cloned.1.call-start = ((), (), s32[]{:S(2)}) async-start(), calls=%async_computation.6 | async-start | bytes 5242880 | tf_op jit(solution)/shard_map/all_gather | solution.py:121
  184.0 1.8 copy-start.1
  184.0 2.3 copy-start.6
  185.6 69.1 %all-reduce.4.cloned.1.call-start = ((), (), s32[]{:S(2)}) async-start(), calls=%async_computation.3 | async-start | bytes 1048576 | tf_op jit(solution)/shard_map/psum | solution.py:68
  185.9 2.4 copy-start.5
  188.3 4.2 %copy-start.4 = (f32[128,4]{0,1:T(4,128)S(1)}, f32[128,4]{0,1:T(4,128)}, u32[]{:S(2)}) copy-start(f32[128,4]{0,1:T(4,128)} %param.24) | copy-start | bytes 6148
  188.3 4.2 %copy-start.2 = (f32[31,384]{1,0:T(8,128)S(1)}, f32[31,384]{1,0:T(8,128)}, u32[]{:S(2)}) copy-start(f32[31,384]{1,0:T(8,128)} %param.18) | copy-start | bytes 142852
  188.3 4.4 %copy-start.3 = (s32[128,4]{0,1:T(4,128)S(1)}, s32[128,4]{0,1:T(4,128)}, u32[]{:S(2)}) copy-start(s32[128,4]{0,1:T(4,128)} %param.23) | copy-start | bytes 6148
  188.3 12.9 %copy-start.7 = (f32[384]{0:T(512)S(1)}, f32[384]{0:T(512)}, u32[]{:S(2)}) copy-start(f32[384]{0:T(512)} %param.19) | copy-start | bytes 4612
  188.9 4.9 %collective-permute-start = (bf16[30,384]{1,0:T(8,128)(2,1)S(1)}, bf16[30,384]{1,0:T(8,128)(2,1)S(1)}, u32[]{:S(2)}, u32[]{:S(2)}) collective-permute-start(bf16[30,384]{1,0:T(8,128)(2,1)S(1)} %slice.260), channel_id=1, source_target_pairs={{0,4},{4,8},{8,12},{12,16},{16,20},{20,24},{24,28},{1,5},{5,9},{9,... | collective-permute-start | bytes 69128 | tf_op jit(solution)/shard_map/ppermute | solution.py:17
Sparse Core Ops, SparseCore 0:
  56.1 33.4 all-gather.2
  106.7 44.5 reduce-scatter.1
  185.7 32.6 all-gather.4
  221.2 33.4 all-reduce.3
where the time goes:
time: 264 us; the launch traced here: 263 us
  waiting for transfers between devices  111 us (42%)
  blocking collectives  70.2 us (27%)
  local copies, waits for them, and re-layouts  26 us (10%)
  matrix products  22.1 us (8%)
  other arithmetic  15.7 us (6%)
  between operations  14 us (5%)
  starting transfers between devices  3.71 us (1%)
    reduce_scatter x1, waiting for transfers between devices, local(): lax.psum_scatter(jnp.dot(hidden, down_w, preferred_element_type=jnp.float...  44.7 us
    all_gather x1, waiting for transfers between devices, local(): block_rows = lax.all_gather(arrived, 'tp', axis=0, tiled=True)  33.6 us
    all_to_all x1, blocking collectives, local(): lax.all_to_all(sending, 'ep', split_axis=1, concat_axis=1, tiled=True)  32.8 us
    all_to_all x1, blocking collectives, local(): lax.all_to_all(summed.reshape(slot_share, experts, width), 'ep', split_ax...  30.9 us
    psum x1, waiting for transfers between devices, local(): lax.psum(jnp.dot(activated, w_output, preferred_element_type=jnp.float32)...  17.7 us
    all_gather x1, waiting for transfers between devices, local(): lax.all_gather(returned, 'tp', axis=0, tiled=True)  14.5 us
    gather x2, local copies, waits for them, and re-layouts, local(): picked = jnp.take(every_slot, slot_index * experts + flat_ids, axis=0)  12.1 us
    dot_general x1, matrix products, local(): jnp.dot(hidden, down_w, preferred_element_type=jnp.float32)  10.3 us
  transfers between devices with their start and end apart: 5, of which 5 were waited for; matrix products, arithmetic and copies ran while one was open for 10% of the time, Pallas kernels for 0%

commit v1 on v0

--- a/solution.py
+++ b/solution.py
@@ -115,8 +115,16 @@
         scatter_dimension=0,
         tiled=True,
     )
-    returned = lax.all_to_all(
-        summed.reshape(slot_share, experts, width), "ep", split_axis=1, concat_axis=1, tiled=True
+    returned = jnp.concatenate(
+        lax.all_to_all(
+            jnp.stack(
+                jnp.split(summed.reshape(slot_share, experts, width), lax.axis_size("ep"), axis=1)
+            ),
+            "ep",
+            0,
+            0,
+        ),
+        axis=1,
     )
     every_slot = lax.all_gather(returned, "tp", axis=0, tiled=True).reshape(
         capacity * experts, width

time: 264 us -> 268 us (1.015)
  local copies, waits for them, and re-layouts: 26 us -> 36.3 us
  waiting for transfers between devices: 111 us -> 105 us
    psum x1, waiting for transfers between devices: 17.7 us -> 11.1 us  [local(): lax.psum(jnp.dot(activated, w_output, preferred_element_type=jnp.float32)...]
    all_gather x0 -> x1, local copies, waits for them, and re-layouts: none -> 6.45 us  [local(): lax.all_gather(returned, 'tp', axis=0, tiled=True)]
    split x0 -> x1, local copies, waits for them, and re-layouts: none -> 6.37 us  [local(): jnp.split(summed.reshape(slot_share, experts, width), lax.axis_size('ep')...]
  transfers between devices with their start and end apart: 5 -> 5, of which waited for: 5 -> 5; matrix products, arithmetic and copies ran while one was open for 10% -> 12% of each run, Pallas kernels for 0% -> 0%
where the time goes in v1:
time: 268 us; the launch traced here: 267 us
  waiting for transfers between devices  105 us (39%)
  blocking collectives  70.4 us (26%)
  local copies, waits for them, and re-layouts  36.3 us (14%)
  matrix products  22.1 us (8%)
  other arithmetic  15.7 us (6%)
  between operations  14.1 us (5%)
  starting transfers between devices  3.71 us (1%)
    reduce_scatter x1, waiting for transfers between devices, local(): lax.psum_scatter(jnp.dot(hidden, down_w, preferred_element_type=jnp.float...  44.5 us
    all_gather x1, waiting for transfers between devices, local(): block_rows = lax.all_gather(arrived, 'tp', axis=0, tiled=True)  33.6 us
    all_to_all x1, blocking collectives, local(): lax.all_to_all(sending, 'ep', split_axis=1, concat_axis=1, tiled=True)  32.8 us
    all_to_all x1, blocking collectives, local(): lax.all_to_all(jnp.stack(jnp.split(summed.reshape(slot_share, experts, wi...  31 us
    all_gather x1, waiting for transfers between devices, local(): lax.all_gather(returned, 'tp', axis=0, tiled=True)  14.8 us
    gather x2, local copies, waits for them, and re-layouts, local(): picked = jnp.take(every_slot, slot_index * experts + flat_ids, axis=0)  12.2 us
    psum x1, waiting for transfers between devices, local(): lax.psum(jnp.dot(activated, w_output, preferred_element_type=jnp.float32)...  11.1 us
    dot_general x1, matrix products, local(): jnp.dot(hidden, down_w, preferred_element_type=jnp.float32)  10.3 us
  transfers between devices with their start and end apart: 5, of which 5 were waited for; matrix products, arithmetic and copies ran while one was open for 12% of the time, Pallas kernels for 0%

profile of v1, /device:TPU:0, one launch (start us, length us, event | category | flops | bytes accessed | tf_op | source)
XLA Modules:
  0.0 267.0 jit_solution(8943383415014041193)
XLA Ops:
  10.0 2.4 scatter_custom_fusion
  13.8 1.3 fusion.24
  15.3 1.4 fusion.26
  16.8 2.3 gather_fusion
  19.1 2.4 copy_select_fusion
  21.6 32.8 %all_to_all.10 = bf16[32,8,2048]{2,0,1:T(8,128)(2,1)S(1)} all-to-all(bf16[32,8,2048]{2,0,1:T(8,128)(2,1)S(1)} %copy_select_fusion), channel_id=1, replica_groups=mesh['ep'=8,'tp'=4] {'ep'}, dimensions={1} | all-to-all | bytes 2097152 | tf_op jit(solution)/shard_map/all_to_all | solution.py:97
  54.4 1.6 copy.64
  56.0 33.6 %all-gather.4.cloned.1.call-done = bf16[128,8,2048]{2,1,0:T(8,128)(2,1)} async-done(((bf16[32,8,2048]{2,1,0:T(8,128)(2,1)}), bf16[128,8,2048]{2,1,0:T(8,128)(2,1)}) %all-gather.4.cloned.1.call-update) | async-done | bytes 4194320 | tf_op jit(solution)/shard_map/all_gather | solution.py:98
  89.7 6.6 %fusion.2 = f32[1024,512]{1,0:T(8,128)} fusion(bf16[128,8,2048]{2,1,0:T(8,128)(2,1)} %all-gather.4.cloned.1.call-done, bf16[1,2048,512]{2,1,0:T(8,128)(2,1)} %param.26), kind=kOutput, calls=%fused_computation.5 | convolution fusion | flops 2147483648 | bytes 8388608 | tf_op jit(solution)/shard_map/dot_general | solution.py:104
  96.2 10.3 %convolution_convert_fusion = bf16[1024,2048]{1,0:T(8,128)(2,1)} fusion(bf16[1,512,2048]{2,1,0:T(8,128)(2,1)S(1)} %copy-done, f32[1024,512]{1,0:T(8,128)} %fusion.2, bf16[1,2048,512]{2,1,0:T(8,128)(2,1)} %param.25, bf16[128,8,2048]{2,1,0:T(8,128)(2,1)} %all-gather.4.cloned.1.call-done), kind=kOutput, calls=%fused_computation.9 | convolution fusion | flops 4302307328 | bytes 14680064 | tf_op jit(solution)/shard_map/dot_general | solution.py:113
  106.8 44.5 %reduce-scatter.2.cloned.1.call-done = bf16[256,2048]{1,0:T(8,128)(2,1)} async-done(((bf16[1024,2048]{1,0:T(8,128)(2,1)}), bf16[256,2048]{1,0:T(8,128)(2,1)}) %reduce-scatter.2.cloned.1.call-update) | async-done | bytes 1048592 | tf_op jit(solution)/shard_map/reduce_scatter | solution.py:112
  151.3 6.4 %fusion.92 = (bf16[32,1,2048]{2,1,0:T(2,128)(2,1)S(1)}, bf16[32,1,2048]{2,1,0:T(2,128)(2,1)S(1)}, bf16[32,1,2048]{2,1,0:T(2,128)(2,1)S(1)}, bf16[32,1,2048]{2,1,...) fusion(bf16[32,8,2048]{2,1,0:T(8,128)(2,1)} %bitcast.82), kind=kLoop, calls=%fused_computation.219 | loop fusion | bytes 2097152 | tf_op jit(solution)/shard_map/split | solution.py:121
  158.4 31.0 %all_to_all.11 = bf16[8,32,1,2048]{3,1,2,0:T(8,128)(2,1)} all-to-all(bf16[8,32,1,2048]{3,1,2,0:T(8,128)(2,1)S(1)} %fusion.34), channel_id=1, replica_groups=mesh['ep'=8,'tp'=4] {'ep'}, dimensions={0} | all-to-all | bytes 2097152 | tf_op jit(solution)/shard_map/all_to_all | solution.py:119
  190.0 1.9 fusion.89
  192.5 3.4 %collective-permute-start = (bf16[30,384]{1,0:T(8,128)(2,1)S(1)}, bf16[30,384]{1,0:T(8,128)(2,1)S(1)}, u32[]{:S(2)}, u32[]{:S(2)}) collective-permute-start(bf16[30,384]{1,0:T(8,128)(2,1)S(1)} %slice.260), channel_id=1, source_target_pairs={{0,4},{4,8},{8,12},{12,16},{16,20},{20,24},{24,28},{1,5},{5,9},{9,... | collective-permute-start | bytes 69128 | tf_op jit(solution)/shard_map/ppermute | solution.py:17
  198.3 6.5 %all-reduce.1 = (f32[128,1]{0,1:T(1,128)S(1)}, f32[128,1]{0,1:T(1,128)S(1)}) all-reduce(f32[128,1]{0,1:T(1,128)S(1)} %bitcast.87, f32[128,1]{0,1:T(1,128)S(1)} %bitcast.86), channel_id=1, replica_groups=mesh['ep'=8,'tp'=4] {'tp'}, use_global_device_ids=true, to_apply=%region_5.0 | all-reduce | flops 256 | bytes 2048 | tf_op jit(solution)/shard_map/psum | solution.py:56
  204.8 2.7 %convolution_convert_fusion.1 = bf16[128,2048]{1,0:T(8,128)(2,1)} fusion(bf16[384,2048]{1,0:T(8,128)(2,1)} %param.20, f32[128,384]{1,0:T(8,128)S(1)} %get-tuple-element.39, f32[384]{0:T(512)S(1)} %copy-done.7, f32[128]{0:T(128)S(1)} %get-tuple-element.49, f32[128]{0:T(128)S(1)} %get-tuple-element.48), kind=kOutput, calls=%fused_computation.10 | convolution fusion | flops 201981952 | bytes 2296320 | tf_op jit(solution)/shard_map/dot_general | solution.py:69
  207.6 14.8 %all-gather.6.cloned.1.call-done = bf16[128,8,1,2048]{3,0,2,1:T(8,128)(2,1)} async-done(((bf16[32,8,1,2048]{3,0,2,1:T(8,128)(2,1)}), bf16[128,8,1,2048]{3,0,2,1:T(8,128)(2,1)}) %all-gather.6.cloned.1.call-update) | async-done | bytes 4194320 | tf_op jit(solution)/shard_map/all_gather | solution.py:129
  222.4 6.5 %copy.109 = bf16[128,8,1,2048]{3,1,0,2:T(8,128)(2,1)} copy(bf16[128,8,1,2048]{3,0,2,1:T(8,128)(2,1)} %all-gather.6.cloned.1.call-done) | data formatting | bytes 8388608 | tf_op jit(solution)/shard_map/all_gather | solution.py:129
  228.8 8.1 %gather_fusion.1 = bf16[512,2048]{1,0:T(8,128)(2,1)} fusion(bf16[1024,2048]{1,0:T(8,128)(2,1)} %bitcast.79, s32[1024]{0:T(1024)S(1)} %pad_clamp_fusion), kind=kCustom, calls=%fused_computation.1 | custom fusion | bytes 4196352 | tf_op jit(solution)/shard_map/jit(_take)/gather | solution.py:132
  236.9 4.1 %gather.15 = bf16[128,4,2048]{2,1,0:T(4,128)(2,1)} reshape(bf16[512,2048]{1,0:T(8,128)(2,1)} %gather_fusion.1) | data formatting | bytes 4194304 | tf_op jit(solution)/shard_map/jit(_take)/gather | solution.py:132
  241.0 6.4 %multiply_reduce_fusion = bf16[128,2048]{1,0:T(8,128)(2,1)} fusion(f32[128,4]{1,0:T(8,128)S(1)} %copy.74, bf16[128,4,2048]{2,1,0:T(4,128)(2,1)} %gather.15, pred[128,4]{1,0:T(8,128)(4,1)S(1)} %copy.60), kind=kLoop, calls=%fused_computation.8 | loop fusion | flops 3932160 | bytes 2624000 | tf_op jit(solution)/shard_map/reduce_sum | solution.py:134
  247.5 11.1 %all-reduce.4.cloned.1.call-done = bf16[128,2048]{1,0:T(8,128)(2,1)} async-done(((bf16[128,2048]{1,0:T(8,128)(2,1)}), bf16[128,2048]{1,0:T(8,128)(2,1)}) %all-reduce.4.cloned.1.call-update) | async-done | bytes 524304 | tf_op jit(solution)/shard_map/psum | solution.py:68
  258.6 1.9 copy.118
  (72 shorter events, 8.8 us)
Async XLA Ops:
  7.2 89.1 %copy-start = (bf16[1,512,2048]{2,1,0:T(8,128)(2,1)S(1)}, bf16[1,512,2048]{2,1,0:T(8,128)(2,1)}, u32[]{:S(2)}) copy-start(bf16[1,512,2048]{2,1,0:T(8,128)(2,1)} %param.27) | copy-start | bytes 6291460
  7.2 82.5 %all-gather.4.cloned.1.call-start = ((), (), s32[]{:S(2)}) async-start(), calls=%async_computation.4 | async-start | bytes 5242880 | tf_op jit(solution)/shard_map/all_gather | solution.py:98
  56.0 95.3 %reduce-scatter.2.cloned.1.call-start = ((), (), s32[]{:S(2)}) async-start(), calls=%async_computation.5 | async-start | bytes 5242880 | tf_op jit(solution)/shard_map/reduce_scatter | solution.py:112
  106.6 115.8 %all-gather.6.cloned.1.call-start = ((), (), s32[]{:S(2)}) async-start(), calls=%async_computation.6 | async-start | bytes 5242880 | tf_op jit(solution)/shard_map/all_gather | solution.py:129
  158.1 31.4 %copy-start.1 = (bf16[128,2048]{1,0:T(8,128)(2,1)S(1)}, bf16[128,2048]{1,0:T(8,128)(2,1)}, u32[]{:S(2)}) copy-start(bf16[128,2048]{1,0:T(8,128)(2,1)} %param.14) | copy-start | bytes 1572868
  158.4 31.6 %copy-start.6 = (f32[2048]{0:T(1024)S(1)}, f32[2048]{0:T(1024)}, u32[]{:S(2)}) copy-start(f32[2048]{0:T(1024)} %param.15) | copy-start | bytes 24580
  189.5 69.1 %all-reduce.4.cloned.1.call-start = ((), (), s32[]{:S(2)}) async-start(), calls=%async_computation.3 | async-start | bytes 1048576 | tf_op jit(solution)/shard_map/psum | solution.py:68
  189.5 2.4 copy-start.5
  191.9 4.2 %copy-start.4 = (f32[128,4]{0,1:T(4,128)S(1)}, f32[128,4]{0,1:T(4,128)}, u32[]{:S(2)}) copy-start(f32[128,4]{0,1:T(4,128)} %param.24) | copy-start | bytes 6148
  191.9 4.2 %copy-start.2 = (f32[31,384]{1,0:T(8,128)S(1)}, f32[31,384]{1,0:T(8,128)}, u32[]{:S(2)}) copy-start(f32[31,384]{1,0:T(8,128)} %param.18) | copy-start | bytes 142852
  191.9 4.4 %copy-start.3 = (s32[128,4]{0,1:T(4,128)S(1)}, s32[128,4]{0,1:T(4,128)}, u32[]{:S(2)}) copy-start(s32[128,4]{0,1:T(4,128)} %param.23) | copy-start | bytes 6148
  192.0 12.9 %copy-start.7 = (f32[384]{0:T(512)S(1)}, f32[384]{0:T(512)}, u32[]{:S(2)}) copy-start(f32[384]{0:T(512)} %param.19) | copy-start | bytes 4612
  192.5 4.9 %collective-permute-start = (bf16[30,384]{1,0:T(8,128)(2,1)S(1)}, bf16[30,384]{1,0:T(8,128)(2,1)S(1)}, u32[]{:S(2)}, u32[]{:S(2)}) collective-permute-start(bf16[30,384]{1,0:T(8,128)(2,1)S(1)} %slice.260), channel_id=1, source_target_pairs={{0,4},{4,8},{8,12},{12,16},{16,20},{20,24},{24,28},{1,5},{5,9},{9,... | collective-permute-start | bytes 69128 | tf_op jit(solution)/shard_map/ppermute | solution.py:17
Sparse Core Ops, SparseCore 0:
  56.1 33.4 all-gather.3
  106.7 44.5 reduce-scatter.1
  189.6 32.7 all-gather.5
  225.1 33.4 all-reduce.3
